TPU v7x, 32 devices: a whole 2x2x4 slice. The times are simulated.
32 devices in a mesh: grp: 2 (over y), sp: 4 (over z), tp: 4 (over x, core).
Axes of the slice: x: 2, y: 2, z: 4, core: 2. Of those that a mesh axis runs over, the one named last changes fastest.
Arguments:
- stream: bfloat16 [6144, 4096], P(('grp', 'sp'), 'tp'), parts along dimension 0, may hold values from -400 to 400
- in_weight: bfloat16 [2, 1024, 4096], P(None, 'sp', 'tp'), may hold values from -0.09375 to 0.09375
- out_weight: bfloat16 [2, 1024, 4096], P(None, 'sp', 'tp'), may hold values from -0.1875 to 0.1875
- group_mix: bfloat16 [2, 4, 256, 256], replicated, may hold values from -0.375 to 0.375
- pool_gain: float32 [2, 1024], replicated, may hold values from 0.1 to 1.9
- norm_gain: float32 [2, 4096], P(None, 'tp'), may hold values from 0.1 to 1.9
- norm_shift: float32 [2, 4096], P(None, 'tp'), may hold values from -3 to 3
Outputs:
- refined: bfloat16 [6144, 4096], P(('grp', 'sp'), 'tp'), parts along dimension 0
There are 2 independent parts, one for each index of `grp`. A program takes and returns all parts, laid end to end along the dimension named above; an argument that names none is the same for every part. Nothing has to cross between parts.
All inputs are finite; a program needn't handle non-finite values.
Results may differ from a plain program's by a relative error of at most 0.015.
Values may be sent and summed in bfloat16 or wider, within the bound.
A program may use at most 64 MiB of HBM per device.

v0:
```python
import jax
import jax.numpy as jnp
from jax import lax
from jax.sharding import PartitionSpec as P

D = 4096
POOL = 1024
GROUPS = 4
GROUP_WIDTH = 256
LAYERS = 2
epsilon = 1e-05


def passed_along(block, axis, distance):
    devices = range(lax.axis_size(axis))
    route = [(i - distance, i) for i in devices if i - distance in devices]
    return lax.ppermute(block, axis, route)


def pooled_windows(hidden, tok_start):
    reach = 2**GROUPS - 1
    length = hidden.shape[1]
    channels = hidden.shape[0]
    earlier = passed_along(hidden[:, length - reach :], "sp", 1)
    extended = jnp.concatenate([earlier, hidden], axis=1).astype(jnp.float32)
    group_ids = (jnp.arange(channels, dtype=jnp.int32) // GROUP_WIDTH)[:, None]
    running = extended
    window_sums = jnp.zeros((channels, length), jnp.float32)
    for octave in range(GROUPS):
        offset = 2**octave
        running = running[:, offset:] + running[:, : running.shape[1] - offset]
        window_sums = jnp.where(
            group_ids == octave, running[:, running.shape[1] - length :], window_sums
        )
    positions = (tok_start + jnp.arange(length, dtype=jnp.int32) + 1).astype(jnp.float32)
    widths = jnp.exp2((group_ids + 1).astype(jnp.float32))
    counts = jnp.minimum(positions[None, :], widths)
    return (window_sums / counts - hidden.astype(jnp.float32)).astype(jnp.bfloat16)


def per_device(stream, in_weight, out_weight, group_mix, pool_gain, norm_gain, norm_shift):
    tok_rows = stream.shape[0]
    tok_start = lax.axis_index("sp") * tok_rows
    alpha = (2.0 * LAYERS) ** 0.25
    contract_rows = (((0,), (0,)), ((), ()))
    contract_cols = (((1,), (1,)), ((), ()))
    current = stream
    for layer_index in range(LAYERS):
        whole_in = lax.all_gather(in_weight[layer_index], "sp", axis=0, tiled=True)
        partial_value = lax.dot_general(
            whole_in, current, contract_cols, preferred_element_type=jnp.float32
        )
        hidden = lax.psum(partial_value.astype(jnp.bfloat16), "tp")
        pooled = pooled_windows(hidden, tok_start)
        grouped = pooled.reshape(GROUPS, GROUP_WIDTH, tok_rows)
        mixed = jnp.einsum(
            "gio,git->got", group_mix[layer_index], grouped, preferred_element_type=jnp.float32
        )
        gains = pool_gain[layer_index].reshape(GROUPS, GROUP_WIDTH, 1)
        scaled = (mixed * gains).astype(jnp.bfloat16).reshape(POOL, tok_rows)
        branch = lax.dot_general(
            scaled,
            lax.all_gather(out_weight[layer_index], "sp", axis=0, tiled=True),
            contract_rows,
            preferred_element_type=jnp.float32,
        )
        summed = alpha * current.astype(jnp.float32) + branch
        row_sum, row_squares = lax.psum(
            (jnp.sum(summed, axis=1), jnp.sum(summed * summed, axis=1)), "tp"
        )
        row_mean = row_sum / D
        row_var = row_squares / D - row_mean * row_mean
        normed = (summed - row_mean[:, None]) * lax.rsqrt(row_var + epsilon)[:, None]
        current = (
            normed * norm_gain[layer_index][None, :] + norm_shift[layer_index][None, :]
        ).astype(jnp.bfloat16)
    return current


def solution(mesh):
    in_specs = (
        P(("grp", "sp"), "tp"),
        P(None, "sp", "tp"),
        P(None, "sp", "tp"),
        P(),
        P(),
        P(None, "tp"),
        P(None, "tp"),
    )
    out_specs = P(("grp", "sp"), "tp")
    return jax.shard_map(
        per_device, mesh=mesh, in_specs=in_specs, out_specs=out_specs, check_vma=False
    )
```

profile of v0, /device:TPU:0, one launch (start us, length us, event | category | flops | bytes accessed | tf_op | source)
XLA Modules:
  0.0 312.8 jit_solution(13905823871252964514)
XLA Ops:
  6.5 2.2 fusion.49
  8.9 48.5 %all-gather.9.cloned.1.call-done = bf16[1,1024,1024]{2,1,0:T(8,128)(2,1)} async-done(((bf16[1,256,1024]{2,1,0:T(8,128)(2,1)}), bf16[1,1024,1024]{2,1,0:T(8,128)(2,1)}) %all-gather.9.cloned.1.call-update) | async-done | bytes 2097168 | tf_op jit(solution)/shard_map/all_gather | solution.py:49
  57.3 5.0 %fusion.22 = bf16[1024,768]{1,0:T(8,128)(2,1)} fusion(bf16[768,1024]{1,0:T(8,128)(2,1)} %param.7, bf16[1,1024,1024]{2,1,0:T(8,128)(2,1)} %all-gather.9.cloned.1.call-done), kind=kOutput, calls=%fused_computation.40 | convolution fusion | flops 1611399168 | bytes 5242880 | tf_op jit(solution)/shard_map/dot_general | solution.py:50
  62.4 1.1 fusion.48
  64.3 39.9 %all-reduce.5.cloned.1.call-done = bf16[1024,768]{1,0:T(8,128)(2,1)} async-done(((bf16[1024,768]{1,0:T(8,128)(2,1)}), bf16[1024,768]{1,0:T(8,128)(2,1)}) %all-reduce.5.cloned.1.call-update) | async-done | bytes 1572880 | tf_op jit(solution)/shard_map/psum | solution.py:53
  104.2 1.1 slice.138
  105.3 3.4 %collective-permute-start = (bf16[1024,15]{1,0:T(8,128)(2,1)S(1)}, bf16[1024,15]{1,0:T(8,128)(2,1)S(1)}, u32[]{:S(2)}, u32[]{:S(2)}) collective-permute-start(bf16[1024,15]{1,0:T(8,128)(2,1)S(1)} %slice.138), channel_id=1, source_target_pairs={{0,4},{4,8},{8,12},{1,5},{5,9},{9,13},{2,6},{6,10},{10,14},{3,7},{... | collective-permute-start | bytes 92168 | tf_op jit(solution)/shard_map/ppermute | solution.py:17
  108.7 5.4 %collective-permute-done = bf16[1024,15]{1,0:T(8,128)(2,1)S(1)} collective-permute-done((bf16[1024,15]{1,0:T(8,128)(2,1)S(1)}, bf16[1024,15]{1,0:T(8,128)(2,1)S(1)}, u32[]{:S(2)}, u32[]{:S(2)}) %collective-permute-start) | collective-permute-done | bytes 30752 | tf_op jit(solution)/shard_map/ppermute | solution.py:17
  114.1 2.3 maximum_convert_fusion
  116.4 1.0 slice_add_fusion.5
  117.4 1.0 slice_add_fusion.4
  118.5 1.0 slice_add_fusion.3
  119.9 4.1 %fusion.1 = bf16[1024,768]{1,0:T(8,128)(2,1)S(1)} fusion(f32[1024,782]{1,0:T(8,128)S(1)} %slice_add_fusion.5, f32[1024,780]{1,0:T(8,128)S(1)} %slice_add_fusion.4, f32[1024,776]{1,0:T(8,128)S(1)} %slice_add_fusion.3, bf16[1024,768]{1,0:T(8,128)(2,1)S(1)} %copy-done, f32[1024]{0:T(1024)S(1)} %fusion.44, f32[768]{0:T(1024)S(1)} %add_convert_fusion.2, ...), kind=kLoop, calls=%fused_computation.9 | loop fusion | flops 7864320 | bytes 15739904 | tf_op jit(solution)/shard_map/convert_element_type | solution.py:38
  124.7 26.8 %all-gather.11.cloned.1.call-done = bf16[1,1024,1024]{2,1,0:T(8,128)(2,1)} async-done(((bf16[1,256,1024]{2,1,0:T(8,128)(2,1)}), bf16[1,1024,1024]{2,1,0:T(8,128)(2,1)}) %all-gather.11.cloned.1.call-update) | async-done | bytes 2097168 | tf_op jit(solution)/shard_map/all_gather | solution.py:63
  151.5 5.8 %fusion.47 = (f32[768]{0:T(1024)S(1)}, f32[768]{0:T(1024)S(1)}, f32[768,1024]{1,0:T(8,128)}) fusion(bf16[1024,768]{1,0:T(8,128)(2,1)S(1)} %bitcast.56, bf16[1,1024,1024]{2,1,0:T(8,128)(2,1)} %all-gather.11.cloned.1.call-done, bf16[768,1024]{1,0:T(8,128)(2,1)} %param.7), kind=kOutput, calls=%fused_computation.70 | convolution fusion | flops 1615329792 | bytes 8394752 | tf_op jit(solution)/shard_map/dot_general | solution.py:61
  157.3 6.5 %all-reduce.1 = (f32[768]{0:T(1024)S(1)}, f32[768]{0:T(1024)S(1)}) all-reduce(f32[768]{0:T(1024)S(1)} %get-tuple-element.8, f32[768]{0:T(1024)S(1)} %get-tuple-element.7), channel_id=1, replica_groups=mesh['grp'=2,'sp'=4,'tp'=4] {'tp'}, use_global_device_ids=true, to_apply=%region_4.5 | all-reduce | flops 1536 | bytes 12288 | tf_op jit(solution)/shard_map/psum | solution.py:68
  163.8 33.6 %all-gather.13.cloned.1.call-done = bf16[1,1024,1024]{2,1,0:T(8,128)(2,1)} async-done(((bf16[1,256,1024]{2,1,0:T(8,128)(2,1)}), bf16[1,1024,1024]{2,1,0:T(8,128)(2,1)}) %all-gather.13.cloned.1.call-update) | async-done | bytes 2097168 | tf_op jit(solution)/shard_map/all_gather | solution.py:49
  197.4 5.6 %fusion.28 = bf16[1024,768]{1,0:T(8,128)(2,1)} fusion(bf16[1,1024,1024]{2,1,0:T(8,128)(2,1)} %all-gather.13.cloned.1.call-done, f32[768,1024]{1,0:T(8,128)} %get-tuple-element.27, f32[1024]{0:T(1024)S(1)} %bitcast.61, f32[1024]{0:T(1024)S(1)} %bitcast.59, f32[768]{0:T(1024)S(1)} %get-tuple-element.26, f32[768]{0:T(1024)S(1)} %get-tuple-element.25), kind=kOutput, calls=%fused_computation.42 | convolution fusion | flops 1615331328 | bytes 6830080 | tf_op jit(solution)/shard_map/dot_general | solution.py:50
  203.7 41.2 %all-reduce.7.cloned.1.call-done = bf16[1024,768]{1,0:T(8,128)(2,1)} async-done(((bf16[1024,768]{1,0:T(8,128)(2,1)}), bf16[1024,768]{1,0:T(8,128)(2,1)}) %all-reduce.7.cloned.1.call-update) | async-done | bytes 1572880 | tf_op jit(solution)/shard_map/psum | solution.py:53
  244.9 1.1 slice.149
  246.0 3.6 %collective-permute-start.1 = (bf16[1024,15]{1,0:T(8,128)(2,1)S(1)}, bf16[1024,15]{1,0:T(8,128)(2,1)S(1)}, u32[]{:S(2)}, u32[]{:S(2)}) collective-permute-start(bf16[1024,15]{1,0:T(8,128)(2,1)S(1)} %slice.149), channel_id=1, source_target_pairs={{0,4},{4,8},{8,12},{1,5},{5,9},{9,13},{2,6},{6,10},{10,14},{3,7},{... | collective-permute-start | bytes 92168 | tf_op jit(solution)/shard_map/ppermute | solution.py:17
  249.6 5.5 %collective-permute-done.1 = bf16[1024,15]{1,0:T(8,128)(2,1)S(1)} collective-permute-done((bf16[1024,15]{1,0:T(8,128)(2,1)S(1)}, bf16[1024,15]{1,0:T(8,128)(2,1)S(1)}, u32[]{:S(2)}, u32[]{:S(2)}) %collective-permute-start.1) | collective-permute-done | bytes 30752 | tf_op jit(solution)/shard_map/ppermute | solution.py:17
  255.2 2.2 maximum_convert_fusion.1
  257.4 1.0 slice_add_fusion.2
  258.4 1.0 slice_add_fusion.1
  259.4 1.0 slice_add_fusion
  260.9 4.1 %fusion.3 = bf16[1024,768]{1,0:T(8,128)(2,1)S(1)} fusion(f32[1024,782]{1,0:T(8,128)S(1)} %slice_add_fusion.2, f32[1024,780]{1,0:T(8,128)S(1)} %slice_add_fusion.1, f32[1024,776]{1,0:T(8,128)S(1)} %slice_add_fusion, bf16[1024,768]{1,0:T(8,128)(2,1)S(1)} %copy-done.1, f32[1024]{0:T(1024)S(1)} %fusion.44, f32[768]{0:T(1024)S(1)} %add_convert_fusion.2, ...), kind=kLoop, calls=%fused_computation.11 | loop fusion | flops 7864320 | bytes 15739904 | tf_op jit(solution)/shard_map/convert_element_type | solution.py:38
  265.0 1.8 multiply_convert_fusion
  266.8 25.3 %all-gather.15.cloned.1.call-done = bf16[1,1024,1024]{2,1,0:T(8,128)(2,1)} async-done(((bf16[1,256,1024]{2,1,0:T(8,128)(2,1)}), bf16[1,1024,1024]{2,1,0:T(8,128)(2,1)}) %all-gather.15.cloned.1.call-update) | async-done | bytes 2097168 | tf_op jit(solution)/shard_map/all_gather | solution.py:63
  292.1 5.6 %fusion.46 = (f32[768]{0:T(1024)S(1)}, f32[768]{0:T(1024)S(1)}, f32[768,1024]{1,0:T(8,128)S(1)}) fusion(bf16[1024,768]{1,0:T(8,128)(2,1)} %bitcast.55, bf16[1,1024,1024]{2,1,0:T(8,128)(2,1)} %all-gather.15.cloned.1.call-done, f32[1024]{0:T(1024)S(1)} %bitcast.62, f32[1024]{0:T(1024)S(1)} %bitcast.60, f32[768]{0:T(1024)S(1)} %get-tuple-element.26, ...), kind=kOutput, calls=%fused_computation.69 | convolution fusion | flops 1619261952 | bytes 9981952 | tf_op jit(solution)/shard_map/dot_general | solution.py:61
  297.7 6.5 %all-reduce = (f32[768]{0:T(1024)S(1)}, f32[768]{0:T(1024)S(1)}) all-reduce(f32[768]{0:T(1024)S(1)} %get-tuple-element.6, f32[768]{0:T(1024)S(1)} %get-tuple-element.5), channel_id=1, replica_groups=mesh['grp'=2,'sp'=4,'tp'=4] {'tp'}, use_global_device_ids=true, to_apply=%region_9.10 | all-reduce | flops 1536 | bytes 12288 | tf_op jit(solution)/shard_map/psum | solution.py:68
  304.2 1.7 add_convert_fusion
  (38 shorter events, 2.9 us)
Async XLA Ops:
  6.5 50.8 %all-gather.9.cloned.1.call-start = ((), (), s32[]{:S(2)}) async-start(), calls=%async_computation.2 | async-start | bytes 2621440 | tf_op jit(solution)/shard_map/all_gather | solution.py:49
  8.8 53.6 %copy-start.2 = (bf16[2,256,1024]{2,1,0:T(8,128)(2,1)S(1)}, bf16[2,256,1024]{2,1,0:T(8,128)(2,1)}, u32[]{:S(2)}) copy-start(bf16[2,256,1024]{2,1,0:T(8,128)(2,1)} %param.9) | copy-start | bytes 3145732
  8.8 95.4 %all-reduce.5.cloned.1.call-start = ((), (), s32[]{:S(2)}) async-start(), calls=%async_computation | async-start | bytes 3145728 | tf_op jit(solution)/shard_map/psum | solution.py:53
  62.3 1.9 copy-start.4
  62.3 1.9 copy-start.5
  62.3 1.9 copy-start.6
  62.4 89.1 %all-gather.11.cloned.1.call-start = ((), (), s32[]{:S(2)}) async-start(), calls=%async_computation.3 | async-start | bytes 2621440 | tf_op jit(solution)/shard_map/all_gather | solution.py:63
  63.5 133.9 %all-gather.13.cloned.1.call-start = ((), (), s32[]{:S(2)}) async-start(), calls=%async_computation.4 | async-start | bytes 2621440 | tf_op jit(solution)/shard_map/all_gather | solution.py:49
  64.1 180.8 %all-reduce.7.cloned.1.call-start = ((), (), s32[]{:S(2)}) async-start(), calls=%async_computation.1 | async-start | bytes 3145728 | tf_op jit(solution)/shard_map/psum | solution.py:53
  105.3 8.8 %collective-permute-start = (bf16[1024,15]{1,0:T(8,128)(2,1)S(1)}, bf16[1024,15]{1,0:T(8,128)(2,1)S(1)}, u32[]{:S(2)}, u32[]{:S(2)}) collective-permute-start(bf16[1024,15]{1,0:T(8,128)(2,1)S(1)} %slice.138), channel_id=1, source_target_pairs={{0,4},{4,8},{8,12},{1,5},{5,9},{9,13},{2,6},{6,10},{10,14},{3,7},{... | collective-permute-start | bytes 92168 | tf_op jit(solution)/shard_map/ppermute | solution.py:17
  118.5 1.4 copy-start
  119.9 4.1 %copy-start.3 = (bf16[2,4,256,256]{3,2,1,0:T(8,128)(2,1)S(1)}, bf16[2,4,256,256]{3,2,1,0:T(8,128)(2,1)}, u32[]{:S(2)}) copy-start(bf16[2,4,256,256]{3,2,1,0:T(8,128)(2,1)} %param.10) | copy-start | bytes 3145732
  203.1 89.0 %all-gather.15.cloned.1.call-start = ((), (), s32[]{:S(2)}) async-start(), calls=%async_computation.5 | async-start | bytes 2621440 | tf_op jit(solution)/shard_map/all_gather | solution.py:63
  246.0 9.2 %collective-permute-start.1 = (bf16[1024,15]{1,0:T(8,128)(2,1)S(1)}, bf16[1024,15]{1,0:T(8,128)(2,1)S(1)}, u32[]{:S(2)}, u32[]{:S(2)}) collective-permute-start(bf16[1024,15]{1,0:T(8,128)(2,1)S(1)} %slice.149), channel_id=1, source_target_pairs={{0,4},{4,8},{8,12},{1,5},{5,9},{9,13},{2,6},{6,10},{10,14},{3,7},{... | collective-permute-start | bytes 92168 | tf_op jit(solution)/shard_map/ppermute | solution.py:17
  259.4 1.4 copy-start.1
Sparse Core Ops, SparseCore 0:
  8.9 48.3 all-gather.8
  62.5 41.6 all-reduce.4
  105.8 45.7 all-gather.10
  152.9 44.4 all-gather.12
  203.2 41.6 all-reduce.6
  246.3 45.7 all-gather.14
where the time goes:
time: 313 us
  waiting for transfers between devices  227 us (73%)
  matrix products  24.5 us (8%)
  other arithmetic  20.6 us (7%)
  between operations  13.7 us (4%)
  blocking collectives  13 us (4%)
  starting transfers between devices  7.2 us (2%)
  local copies, waits for them, and re-layouts  6.35 us (2%)
    all_gather x2, waiting for transfers between devices, per_device(): whole_in = lax.all_gather(in_weight[layer_index], 'sp', axis=0, tiled=True)  82.1 us
    psum x2, waiting for transfers between devices, per_device(): hidden = lax.psum(partial_value.astype(jnp.bfloat16), 'tp')  81.1 us
    all_gather x2, waiting for transfers between devices, per_device(): lax.all_gather(out_weight[layer_index], 'sp', axis=0, tiled=True)  52.2 us
    psum x2, blocking collectives, per_device(): lax.psum((jnp.sum(summed, axis=1), jnp.sum(summed * summed, axis=1)), 'tp')  13 us
    dot_general x2, matrix products, per_device(): lax.dot_general(scaled, lax.all_gather(out_weight[layer_index], 'sp', axi...  11.4 us
    ppermute x2, waiting for transfers between devices, passed_along(): return lax.ppermute(block, axis, route)  10.9 us
    dot_general x2, matrix products, per_device(): lax.dot_general(whole_in, current, contract_cols, preferred_element_type=...  10.6 us
    convert_element_type x2, other arithmetic, pooled_windows(): (window_sums / counts - hidden.astype(jnp.float32)).astype(jnp.bfloat16)  8.26 us
  transfers between devices with their start and end apart: 8, of which 8 were waited for; matrix products, arithmetic and copies ran while one was open for 10% of the time, Pallas kernels for 0%

commit v1 on v0

--- a/solution.py
+++ b/solution.py
@@ -9,6 +9,17 @@
 GROUP_WIDTH = 256
 LAYERS = 2
 epsilon = 1e-05
+
+
+def turned_line(x, name, d):
+    size = lax.axis_size(name)
+    route = [(i, (i + 1) % size) for i in range(size)]
+    terms = [x]
+    for reach in range(1, size):
+        terms = [lax.ppermute(terms[0], name, route), *terms]
+    whole = jnp.concatenate(terms, axis=d)
+    shift = (lax.axis_index(name) + 1) * terms[-1].shape[d]
+    return jnp.roll(whole, shift, axis=d)
 
 
 def passed_along(block, axis, distance):
@@ -46,7 +57,7 @@
     contract_cols = (((1,), (1,)), ((), ()))
     current = stream
     for layer_index in range(LAYERS):
-        whole_in = lax.all_gather(in_weight[layer_index], "sp", axis=0, tiled=True)
+        whole_in = turned_line(in_weight[layer_index], "sp", 0)
         partial_value = lax.dot_general(
             whole_in, current, contract_cols, preferred_element_type=jnp.float32
         )

time: 313 us -> 240 us (0.77)
  waiting for transfers between devices: 227 us -> 142 us
  matrix products: 24.5 us -> 30.7 us
  starting transfers between devices: 7.2 us -> 12.1 us
    all_gather x2 -> x0, waiting for transfers between devices: 82.1 us -> none  [per_device(): whole_in = lax.all_gather(in_weight[layer_index], 'sp', axis=0, tiled=True)]
    ppermute x0 -> x6, waiting for transfers between devices: none -> 55 us  [turned_line(): terms = [lax.ppermute(terms[0], name, route), *terms]]
    all_gather x2, waiting for transfers between devices: 52.2 us -> 0.03 us  [per_device(): lax.all_gather(out_weight[layer_index], 'sp', axis=0, tiled=True)]
    psum x2, waiting for transfers between devices: 81.1 us -> 70.6 us  [per_device(): hidden = lax.psum(partial_value.astype(jnp.bfloat16), 'tp')]
    dot_general x2, matrix products: 10.6 us -> 16.9 us  [per_device(): lax.dot_general(whole_in, current, contract_cols, preferred_element_type=...]
    ppermute x0 -> x6, starting transfers between devices: none -> 4.87 us  [turned_line(): terms = [lax.ppermute(terms[0], name, route), *terms]]
    ppermute x2, waiting for transfers between devices: 10.9 us -> 15.7 us  [passed_along(): return lax.ppermute(block, axis, route)]
  transfers between devices with their start and end apart: 8 -> 12, of which waited for: 8 -> 8; matrix products, arithmetic and copies ran while one was open for 10% -> 13% of each run, Pallas kernels for 0% -> 0%
where the time goes in v1:
time: 240 us; the launch traced here: 239 us
  waiting for transfers between devices  142 us (59%)
  matrix products  30.7 us (13%)
  other arithmetic  20.6 us (9%)
  between operations  15.1 us (6%)
  blocking collectives  13.4 us (6%)
  starting transfers between devices  12.1 us (5%)
  local copies, waits for them, and re-layouts  5.33 us (2%)
    psum x2, waiting for transfers between devices, per_device(): hidden = lax.psum(partial_value.astype(jnp.bfloat16), 'tp')  70.6 us
    ppermute x6, waiting for transfers between devices, turned_line(): terms = [lax.ppermute(terms[0], name, route), *terms]  55 us
    dot_general x2, matrix products, per_device(): lax.dot_general(whole_in, current, contract_cols, preferred_element_type=...  16.9 us
    ppermute x2, waiting for transfers between devices, passed_along(): return lax.ppermute(block, axis, route)  15.7 us
    psum x2, blocking collectives, per_device(): lax.psum((jnp.sum(summed, axis=1), jnp.sum(summed * summed, axis=1)), 'tp')  13.4 us
    dot_general x2, matrix products, per_device(): lax.dot_general(scaled, lax.all_gather(out_weight[layer_index], 'sp', axi...  11.4 us
    convert_element_type x2, other arithmetic, pooled_windows(): (window_sums / counts - hidden.astype(jnp.float32)).astype(jnp.bfloat16)  8.29 us
    ppermute x2, starting transfers between devices, passed_along(): return lax.ppermute(block, axis, route)  7.08 us
  transfers between devices with their start and end apart: 12, of which 8 were waited for; matrix products, arithmetic and copies ran while one was open for 13% of the time, Pallas kernels for 0%

profile of v1, /device:TPU:0, one launch (start us, length us, event | category | flops | bytes accessed | tf_op | source)
XLA Modules:
  0.0 239.2 jit_solution(1183349852780370681)
XLA Ops:
  7.4 1.3 slice_bitcast_fusion.1
  8.6 3.1 %collective-permute-start = (bf16[256,1024]{1,0:T(8,128)(2,1)S(1)}, bf16[256,1024]{1,0:T(8,128)(2,1)S(1)}, u32[]{:S(2)}, u32[]{:S(2)}) collective-permute-start(bf16[256,1024]{1,0:T(8,128)(2,1)S(1)} %get-tuple-element.18), channel_id=1, source_target_pairs={{0,4},{4,8},{8,12},{12,0},{1,5},{5,9},{9,13},{13,1},{2,6},{6,10},{... | collective-permute-start | bytes 1572872 | tf_op jit(solution)/shard_map/ppermute | solution.py:19
  11.7 13.9 %collective-permute-done = bf16[256,1024]{1,0:T(8,128)(2,1)S(1)} collective-permute-done((bf16[256,1024]{1,0:T(8,128)(2,1)S(1)}, bf16[256,1024]{1,0:T(8,128)(2,1)S(1)}, u32[]{:S(2)}, u32[]{:S(2)}) %collective-permute-start) | collective-permute-done | bytes 524320 | tf_op jit(solution)/shard_map/ppermute | solution.py:19
  25.7 14.9 %collective-permute-done.1 = bf16[256,1024]{1,0:T(8,128)(2,1)S(1)} collective-permute-done((bf16[256,1024]{1,0:T(8,128)(2,1)S(1)}, bf16[256,1024]{1,0:T(8,128)(2,1)S(1)}, u32[]{:S(2)}, u32[]{:S(2)}) %collective-permute-start.1) | collective-permute-done | bytes 524320 | tf_op jit(solution)/shard_map/ppermute | solution.py:19
  40.6 14.1 %collective-permute-done.2 = bf16[256,1024]{1,0:T(8,128)(2,1)} collective-permute-done((bf16[256,1024]{1,0:T(8,128)(2,1)S(1)}, bf16[256,1024]{1,0:T(8,128)(2,1)}, u32[]{:S(2)}, u32[]{:S(2)}) %collective-permute-start.2) | collective-permute-done | bytes 524320 | tf_op jit(solution)/shard_map/ppermute | solution.py:19
  54.7 8.5 %fusion.38 = bf16[1024,768]{1,0:T(8,128)(2,1)} fusion(bf16[768,1024]{1,0:T(8,128)(2,1)} %param.9, s32[]{:T(128)S(6)} %select_n.85, bf16[256,1024]{1,0:T(8,128)(2,1)} %collective-permute-done.2, bf16[256,1024]{1,0:T(8,128)(2,1)S(1)} %collective-permute-done.1, bf16[256,1024]{1,0:T(8,128)(2,1)S(1)} %collective-permute-done, ...), kind=kOutput, calls=%fused_computation.68 | convolution fusion | flops 1628176384 | bytes 5242884 | tf_op jit(solution)/shard_map/dot_general | solution.py:61
  63.4 1.0 fusion.65
  64.6 12.0 %collective-permute-done.4 = bf16[256,1024]{1,0:T(8,128)(2,1)S(1)} collective-permute-done((bf16[256,1024]{1,0:T(8,128)(2,1)S(1)}, bf16[256,1024]{1,0:T(8,128)(2,1)S(1)}, u32[]{:S(2)}, u32[]{:S(2)}) %collective-permute-start.4) | collective-permute-done | bytes 524320 | tf_op jit(solution)/shard_map/ppermute | solution.py:19
  76.6 27.4 %all-reduce.5.cloned.1.call-done = bf16[1024,768]{1,0:T(8,128)(2,1)} async-done(((bf16[1024,768]{1,0:T(8,128)(2,1)}), bf16[1024,768]{1,0:T(8,128)(2,1)}) %all-reduce.5.cloned.1.call-update) | async-done | bytes 1572880 | tf_op jit(solution)/shard_map/psum | solution.py:64
  104.0 1.1 slice.138
  105.1 3.4 %collective-permute-start.3 = (bf16[1024,15]{1,0:T(8,128)(2,1)S(1)}, bf16[1024,15]{1,0:T(8,128)(2,1)S(1)}, u32[]{:S(2)}, u32[]{:S(2)}) collective-permute-start(bf16[1024,15]{1,0:T(8,128)(2,1)S(1)} %slice.138), channel_id=1, source_target_pairs={{0,4},{4,8},{8,12},{1,5},{5,9},{9,13},{2,6},{6,10},{10,14},{3,7},{... | collective-permute-start | bytes 92168 | tf_op jit(solution)/shard_map/ppermute | solution.py:28
  108.5 1.7 collective-permute-start.6
  110.2 10.5 %collective-permute-done.3 = bf16[1024,15]{1,0:T(8,128)(2,1)S(1)} collective-permute-done((bf16[1024,15]{1,0:T(8,128)(2,1)S(1)}, bf16[1024,15]{1,0:T(8,128)(2,1)S(1)}, u32[]{:S(2)}, u32[]{:S(2)}) %collective-permute-start.3) | collective-permute-done | bytes 30752 | tf_op jit(solution)/shard_map/ppermute | solution.py:28
  120.8 2.2 maximum_convert_fusion
  123.0 1.0 slice_add_fusion.5
  124.1 1.0 slice_add_fusion.4
  125.1 1.0 slice_add_fusion.3
  126.5 4.1 %fusion.1 = bf16[1024,768]{1,0:T(8,128)(2,1)S(1)} fusion(f32[1024,782]{1,0:T(8,128)S(1)} %slice_add_fusion.5, f32[1024,780]{1,0:T(8,128)S(1)} %slice_add_fusion.4, f32[1024,776]{1,0:T(8,128)S(1)} %slice_add_fusion.3, bf16[1024,768]{1,0:T(8,128)(2,1)S(1)} %copy-done, f32[1024]{0:T(1024)S(1)} %fusion.57, f32[768]{0:T(1024)S(1)} %add_convert_fusion.2, ...), kind=kLoop, calls=%fused_computation.25 | loop fusion | flops 7864320 | bytes 15739904 | tf_op jit(solution)/shard_map/convert_element_type | solution.py:49
  131.3 5.8 %fusion.64 = (f32[768]{0:T(1024)S(1)}, f32[768]{0:T(1024)S(1)}, f32[768,1024]{1,0:T(8,128)}) fusion(bf16[1024,768]{1,0:T(8,128)(2,1)S(1)} %bitcast.46, bf16[1,1024,1024]{2,1,0:T(8,128)(2,1)} %all-gather.5.cloned.1.call-done, bf16[768,1024]{1,0:T(8,128)(2,1)} %param.9), kind=kOutput, calls=%fused_computation.103 | convolution fusion | flops 1615329792 | bytes 8394752 | tf_op jit(solution)/shard_map/dot_general | solution.py:72
  137.1 7.3 %all-reduce.1 = (f32[768]{0:T(1024)S(1)}, f32[768]{0:T(1024)S(1)}) all-reduce(f32[768]{0:T(1024)S(1)} %get-tuple-element.9, f32[768]{0:T(1024)S(1)} %get-tuple-element.8), channel_id=1, replica_groups=mesh['grp'=2,'sp'=4,'tp'=4] {'tp'}, use_global_device_ids=true, to_apply=%region_4.6 | all-reduce | flops 1536 | bytes 12288 | tf_op jit(solution)/shard_map/psum | solution.py:79
  144.5 8.4 %fusion.41 = bf16[1024,768]{1,0:T(8,128)(2,1)} fusion(s32[]{:T(128)S(6)} %select_n.85, bf16[256,1024]{1,0:T(8,128)(2,1)} %collective-permute-done.6, bf16[256,1024]{1,0:T(8,128)(2,1)} %collective-permute-done.5, bf16[256,1024]{1,0:T(8,128)(2,1)} %copy-done.7, bf16[256,1024]{1,0:T(8,128)(2,1)S(1)} %get-tuple-element.19, f32[768,1024]{1,0:T(8,128)} %get-tuple-element.28, ...), kind=kOutput, calls=%fused_computation.69 | convolution fusion | flops 1632108544 | bytes 6830084 | tf_op jit(solution)/shard_map/dot_general | solution.py:61
  153.5 43.2 %all-reduce.7.cloned.1.call-done = bf16[1024,768]{1,0:T(8,128)(2,1)} async-done(((bf16[1024,768]{1,0:T(8,128)(2,1)}), bf16[1024,768]{1,0:T(8,128)(2,1)}) %all-reduce.7.cloned.1.call-update) | async-done | bytes 1572880 | tf_op jit(solution)/shard_map/psum | solution.py:64
  196.8 1.1 slice.149
  197.9 3.7 %collective-permute-start.7 = (bf16[1024,15]{1,0:T(8,128)(2,1)S(1)}, bf16[1024,15]{1,0:T(8,128)(2,1)S(1)}, u32[]{:S(2)}, u32[]{:S(2)}) collective-permute-start(bf16[1024,15]{1,0:T(8,128)(2,1)S(1)} %slice.149), channel_id=1, source_target_pairs={{0,4},{4,8},{8,12},{1,5},{5,9},{9,13},{2,6},{6,10},{10,14},{3,7},{... | collective-permute-start | bytes 92168 | tf_op jit(solution)/shard_map/ppermute | solution.py:28
  201.6 5.1 %collective-permute-done.7 = bf16[1024,15]{1,0:T(8,128)(2,1)S(1)} collective-permute-done((bf16[1024,15]{1,0:T(8,128)(2,1)S(1)}, bf16[1024,15]{1,0:T(8,128)(2,1)S(1)}, u32[]{:S(2)}, u32[]{:S(2)}) %collective-permute-start.7) | collective-permute-done | bytes 30752 | tf_op jit(solution)/shard_map/ppermute | solution.py:28
  206.7 2.2 maximum_convert_fusion.1
  208.9 1.0 slice_add_fusion.2
  212.4 4.1 %fusion.3 = bf16[1024,768]{1,0:T(8,128)(2,1)S(1)} fusion(f32[1024,782]{1,0:T(8,128)S(1)} %slice_add_fusion.2, f32[1024,780]{1,0:T(8,128)S(1)} %slice_add_fusion.1, f32[1024,776]{1,0:T(8,128)S(1)} %slice_add_fusion, bf16[1024,768]{1,0:T(8,128)(2,1)S(1)} %copy-done.1, f32[1024]{0:T(1024)S(1)} %fusion.57, f32[768]{0:T(1024)S(1)} %add_convert_fusion.2, ...), kind=kLoop, calls=%fused_computation.27 | loop fusion | flops 7864320 | bytes 15739904 | tf_op jit(solution)/shard_map/convert_element_type | solution.py:49
  216.5 1.8 multiply_convert_fusion
  218.3 5.6 %fusion.63 = (f32[768]{0:T(1024)S(1)}, f32[768]{0:T(1024)S(1)}, f32[768,1024]{1,0:T(8,128)S(1)}) fusion(bf16[1024,768]{1,0:T(8,128)(2,1)} %bitcast.45, bf16[1,1024,1024]{2,1,0:T(8,128)(2,1)} %all-gather.7.cloned.1.call-done, f32[1024]{0:T(1024)S(1)} %bitcast.52, f32[1024]{0:T(1024)S(1)} %bitcast.50, f32[768]{0:T(1024)S(1)} %get-tuple-element.27, ...), kind=kOutput, calls=%fused_computation.102 | convolution fusion | flops 1619261952 | bytes 9981952 | tf_op jit(solution)/shard_map/dot_general | solution.py:72
  224.0 6.1 %all-reduce = (f32[768]{0:T(1024)S(1)}, f32[768]{0:T(1024)S(1)}) all-reduce(f32[768]{0:T(1024)S(1)} %get-tuple-element.7, f32[768]{0:T(1024)S(1)} %get-tuple-element.6), channel_id=1, replica_groups=mesh['grp'=2,'sp'=4,'tp'=4] {'tp'}, use_global_device_ids=true, to_apply=%region_9.11 | all-reduce | flops 1536 | bytes 12288 | tf_op jit(solution)/shard_map/psum | solution.py:79
  230.1 1.7 add_convert_fusion
  (46 shorter events, 4.4 us)
Async XLA Ops:
  7.4 96.6 %all-reduce.5.cloned.1.call-start = ((), (), s32[]{:S(2)}) async-start(), calls=%async_computation | async-start | bytes 3145728 | tf_op jit(solution)/shard_map/psum | solution.py:64
  8.6 17.1 %collective-permute-start = (bf16[256,1024]{1,0:T(8,128)(2,1)S(1)}, bf16[256,1024]{1,0:T(8,128)(2,1)S(1)}, u32[]{:S(2)}, u32[]{:S(2)}) collective-permute-start(bf16[256,1024]{1,0:T(8,128)(2,1)S(1)} %get-tuple-element.18), channel_id=1, source_target_pairs={{0,4},{4,8},{8,12},{12,0},{1,5},{5,9},{9,13},{13,1},{2,6},{6,10},{... | collective-permute-start | bytes 1572872 | tf_op jit(solution)/shard_map/ppermute | solution.py:19
  25.7 14.9 %collective-permute-start.1 = (bf16[256,1024]{1,0:T(8,128)(2,1)S(1)}, bf16[256,1024]{1,0:T(8,128)(2,1)S(1)}, u32[]{:S(2)}, u32[]{:S(2)}) collective-permute-start(bf16[256,1024]{1,0:T(8,128)(2,1)S(1)} %collective-permute-done), channel_id=1, source_target_pairs={{0,4},{4,8},{8,12},{12,0},{1,5},{5,9},{9,13},{13,1},{2,6},{6,10},{... | collective-permute-start | bytes 1572872 | tf_op jit(solution)/shard_map/ppermute | solution.py:19
  40.6 14.1 %collective-permute-start.2 = (bf16[256,1024]{1,0:T(8,128)(2,1)S(1)}, bf16[256,1024]{1,0:T(8,128)(2,1)}, u32[]{:S(2)}, u32[]{:S(2)}) collective-permute-start(bf16[256,1024]{1,0:T(8,128)(2,1)S(1)} %collective-permute-done.1), channel_id=1, source_target_pairs={{0,4},{4,8},{8,12},{12,0},{1,5},{5,9},{9,13},{13,1},{2,6},{6,10},{... | collective-permute-start | bytes 1572872 | tf_op jit(solution)/shard_map/ppermute | solution.py:19
  40.6 22.8 %copy-start.2 = (bf16[2,256,1024]{2,1,0:T(8,128)(2,1)S(1)}, bf16[2,256,1024]{2,1,0:T(8,128)(2,1)}, u32[]{:S(2)}) copy-start(bf16[2,256,1024]{2,1,0:T(8,128)(2,1)} %param.11) | copy-start | bytes 3145732
  63.2 1.3 copy-start.4
  63.2 1.3 copy-start.5
  63.2 13.4 %copy-start.6 = (f32[2,1024]{1,0:T(2,128)S(1)}, f32[2,1024]{1,0:T(2,128)}, u32[]{:S(2)}) copy-start(f32[2,1024]{1,0:T(2,128)} %param.15) | copy-start | bytes 24580
  63.2 68.1 %all-gather.5.cloned.1.call-start = ((), (), s32[]{:S(2)}) async-start(), calls=%async_computation.2 | async-start | bytes 2621440 | tf_op jit(solution)/shard_map/all_gather | solution.py:74
  63.3 13.3 %collective-permute-start.4 = (bf16[256,1024]{1,0:T(8,128)(2,1)S(1)}, bf16[256,1024]{1,0:T(8,128)(2,1)S(1)}, u32[]{:S(2)}, u32[]{:S(2)}) collective-permute-start(bf16[256,1024]{1,0:T(8,128)(2,1)S(1)} %get-tuple-element.19), channel_id=1, source_target_pairs={{0,4},{4,8},{8,12},{12,0},{1,5},{5,9},{9,13},{13,1},{2,6},{6,10},{... | collective-permute-start | bytes 1572872 | tf_op jit(solution)/shard_map/ppermute | solution.py:19
  64.4 132.3 %all-reduce.7.cloned.1.call-start = ((), (), s32[]{:S(2)}) async-start(), calls=%async_computation.1 | async-start | bytes 3145728 | tf_op jit(solution)/shard_map/psum | solution.py:64
  76.6 47.5 %copy-start.7 = (bf16[256,1024]{1,0:T(8,128)(2,1)}, bf16[256,1024]{1,0:T(8,128)(2,1)S(1)}, u32[]{:S(2)}) copy-start(bf16[256,1024]{1,0:T(8,128)(2,1)S(1)} %collective-permute-done.4) | copy-start | bytes 1572868
  76.6 32.0 %collective-permute-start.5 = (bf16[256,1024]{1,0:T(8,128)(2,1)S(1)}, bf16[256,1024]{1,0:T(8,128)(2,1)}, u32[]{:S(2)}, u32[]{:S(2)}) collective-permute-start(bf16[256,1024]{1,0:T(8,128)(2,1)S(1)} %collective-permute-done.4), channel_id=1, source_target_pairs={{0,4},{4,8},{8,12},{12,0},{1,5},{5,9},{9,13},{13,1},{2,6},{6,10},{... | collective-permute-start | bytes 1572872 | tf_op jit(solution)/shard_map/ppermute | solution.py:19
  105.1 15.7 %collective-permute-start.3 = (bf16[1024,15]{1,0:T(8,128)(2,1)S(1)}, bf16[1024,15]{1,0:T(8,128)(2,1)S(1)}, u32[]{:S(2)}, u32[]{:S(2)}) collective-permute-start(bf16[1024,15]{1,0:T(8,128)(2,1)S(1)} %slice.138), channel_id=1, source_target_pairs={{0,4},{4,8},{8,12},{1,5},{5,9},{9,13},{2,6},{6,10},{10,14},{3,7},{... | collective-permute-start | bytes 92168 | tf_op jit(solution)/shard_map/ppermute | solution.py:28
  108.5 35.9 %collective-permute-start.6 = (bf16[256,1024]{1,0:T(8,128)(2,1)}, bf16[256,1024]{1,0:T(8,128)(2,1)}, u32[]{:S(2)}, u32[]{:S(2)}) collective-permute-start(bf16[256,1024]{1,0:T(8,128)(2,1)} %collective-permute-done.5), channel_id=1, source_target_pairs={{0,4},{4,8},{8,12},{12,0},{1,5},{5,9},{9,13},{13,1},{2,6},{6,10},{... | collective-permute-start | bytes 1572872 | tf_op jit(solution)/shard_map/ppermute | solution.py:19
  125.1 1.4 copy-start
  126.5 4.2 %copy-start.3 = (bf16[2,4,256,256]{3,2,1,0:T(8,128)(2,1)S(1)}, bf16[2,4,256,256]{3,2,1,0:T(8,128)(2,1)}, u32[]{:S(2)}) copy-start(bf16[2,4,256,256]{3,2,1,0:T(8,128)(2,1)} %param.12) | copy-start | bytes 3145732
  152.9 65.4 %all-gather.7.cloned.1.call-start = ((), (), s32[]{:S(2)}) async-start(), calls=%async_computation.3 | async-start | bytes 2621440 | tf_op jit(solution)/shard_map/all_gather | solution.py:74
  197.9 8.8 %collective-permute-start.7 = (bf16[1024,15]{1,0:T(8,128)(2,1)S(1)}, bf16[1024,15]{1,0:T(8,128)(2,1)S(1)}, u32[]{:S(2)}, u32[]{:S(2)}) collective-permute-start(bf16[1024,15]{1,0:T(8,128)(2,1)S(1)} %slice.149), channel_id=1, source_target_pairs={{0,4},{4,8},{8,12},{1,5},{5,9},{9,13},{2,6},{6,10},{10,14},{3,7},{... | collective-permute-start | bytes 92168 | tf_op jit(solution)/shard_map/ppermute | solution.py:28
  211.0 1.4 copy-start.1
Sparse Core Ops, SparseCore 0:
  63.4 40.6 all-reduce.4
  153.1 43.6 all-reduce.6
Sparse Core Ops, SparseCore 1:
  65.3 65.8 all-gather.4
  155.0 46.3 all-gather.6
